TPU v7x, 32 devices: a whole 2x2x4 slice. The times are simulated.
32 devices in a mesh: sp: 16 (over z, y, x), tp: 2 (over core).
Axes of the slice: x: 2, y: 2, z: 4, core: 2. Of those that a mesh axis runs over, the one named last changes fastest.
Arguments:
- residual: bfloat16 [2048, 2048], P(('sp', 'tp')), may hold values from -6 to 6
- query_wide: bfloat16 [2048, 1024], P('sp', 'tp'), may hold values from -6 to 6
- key_wide: bfloat16 [2048, 1024], P('sp', 'tp'), may hold values from -6 to 6
- value_wide: bfloat16 [2048, 2048], P('sp', 'tp'), may hold values from -6 to 6
- outgate_wide: bfloat16 [2048, 2048], P('sp', 'tp'), may hold values from -6 to 6
- gating_wide: float32 [3, 8, 2048], P(None, 'tp', 'sp'), may hold values from -4 to 240, as said below
- gain_wide: bfloat16 [2048], P('tp'), may hold values from 0.099609375 to 1.8984375
- readout_wide: bfloat16 [2048, 2048], P('tp'), may hold values from -0.109375 to 0.109375
- query_narrow: bfloat16 [2048, 512], P('sp', 'tp'), may hold values from -6 to 6
- key_narrow: bfloat16 [2048, 512], P('sp', 'tp'), may hold values from -6 to 6
- value_narrow: bfloat16 [2048, 1024], P('sp', 'tp'), may hold values from -6 to 6
- outgate_narrow: bfloat16 [2048, 1024], P('sp', 'tp'), may hold values from -6 to 6
- gating_narrow: float32 [3, 8, 2048], P(None, 'tp', 'sp'), may hold values from -4 to 240, as said below
- gain_narrow: bfloat16 [1024], P('tp'), may hold values from 0.099609375 to 1.8984375
- readout_narrow: bfloat16 [1024, 2048], P('tp'), may hold values from -0.109375 to 0.109375
- norm_gain: bfloat16 [2048], replicated, may hold values from 0.099609375 to 1.8984375
- gate_weight: bfloat16 [2048, 5632], P('sp', 'tp'), may hold values from -0.125 to 0.125
- up_weight: bfloat16 [2048, 5632], P('sp', 'tp'), may hold values from -0.125 to 0.125
- down_weight: bfloat16 [5632, 2048], P('tp', 'sp'), may hold values from -0.078125 to 0.078125
Outputs:
- mixed_out: bfloat16 [2048, 2048], P(('sp', 'tp'))
Inputs may be any that keep to these rules, and one draw needn't show every extreme that they name: `gating_wide`: row 0 holds input gate pre-activations, row 1 forget gate pre-activations, row 2 an added log-decay that is zero or negative. `gating_narrow`: row 0 holds input gate pre-activations, row 1 forget gate pre-activations, row 2 an added log-decay that is zero or negative.
All inputs are finite; a program needn't handle non-finite values.
Results may differ from a plain program's by a relative error of at most 0.017.
Values may be sent and summed in bfloat16 or wider, within the bound.
No kernel may reach another device: no remote copies, remote signals or barrier semaphores. Data moves between devices by JAX's collectives and lax.ppermute only.
A program may use at most 128 MiB of HBM per device.

v0:
```python
import jax
import jax.numpy as jnp
from jax import lax
from jax.sharding import PartitionSpec as P

DK_A = 128
DK_B = 64
BLOCK = 64


def entering(value, axis, combine, identity):
    length, here = (lax.axis_size(axis), lax.axis_index(axis))
    everything = jax.tree.map(lambda part: lax.all_gather(part, axis), value)
    start = jax.tree.map(
        lambda part, zero: jnp.broadcast_to(jnp.asarray(zero, part.dtype), part.shape),
        value,
        identity,
    )

    def step(k, before):
        reached = k < here
        new = combine(before, jax.tree.map(lambda part: part[k], everything))
        return jax.tree.map(lambda a, b: jnp.where(reached, a, b), new, before)

    return lax.fori_loop(0, length, step, start)


def local_pass(query, key_rows, value, gating, key_size):
    rows = query.shape[0]
    attention_tally = gating.shape[1]
    value_size = value.shape[1] // attention_tally
    nblocks = rows // BLOCK
    scale = key_size ** (-0.5)
    queries = query.reshape(nblocks, BLOCK, attention_tally, key_size)
    keys_all = key_rows.reshape(nblocks, BLOCK, attention_tally, key_size)
    values_all = value.reshape(nblocks, BLOCK, attention_tally, value_size)
    incoming_matrix = jnp.moveaxis(gating[0].reshape(attention_tally, nblocks, BLOCK), 1, 0)
    forget_log = jax.nn.log_sigmoid(gating[1]) + gating[2]
    forgets = jnp.moveaxis(forget_log.reshape(attention_tally, nblocks, BLOCK), 1, 0)
    causal = jnp.tril(jnp.ones((BLOCK, BLOCK), dtype=bool))

    def advance(carry, blocks):
        memory, level = carry
        q_block, k_block, v_block, in_block, f_block = blocks
        cumul = jnp.cumsum(f_block, axis=-1)
        logits = cumul[:, :, None] - cumul[:, None, :] + in_block[:, None, :]
        logits = jnp.where(causal, logits, -jnp.inf)
        carried = cumul + level[:, None]
        stab = jnp.maximum(carried, jnp.max(logits, axis=-1))
        weights = jnp.exp(logits - stab[:, :, None])
        scores = (
            jnp.einsum("thd,shd->hts", q_block, k_block, preferred_element_type=jnp.float32) * scale
        )
        weighted = (scores * weights).astype(jnp.bfloat16)
        within = jnp.einsum("hts,shv->thv", weighted, v_block, preferred_element_type=jnp.float32)
        earlier = jnp.einsum(
            "thd,hdv->thv", q_block.astype(jnp.float32), memory, precision=lax.Precision.HIGHEST
        )
        earlier = earlier * jnp.exp(carried - stab).T[:, :, None]
        last = cumul[:, -1]
        tail = last[:, None] - cumul + in_block
        level_new = jnp.maximum(last + level, jnp.max(tail, axis=-1))
        tail_weights = jnp.exp(tail - level_new[:, None]) * scale
        scaled_keys = (k_block * tail_weights.T[:, :, None]).astype(jnp.bfloat16)
        memory_new = jnp.exp(last + level - level_new)[:, None, None] * memory
        memory_new = memory_new + jnp.einsum(
            "shd,shv->hdv", scaled_keys, v_block, preferred_element_type=jnp.float32
        )
        return ((memory_new, level_new), (within + earlier, stab))

    init = (
        jnp.zeros((attention_tally, key_size, value_size), jnp.float32),
        jnp.full((attention_tally,), -1e30, jnp.float32),
    )
    (memory_end, level_end), (raw, stabs) = lax.scan(
        advance, init, (queries, keys_all, values_all, incoming_matrix, forgets)
    )
    raw = raw.reshape(rows, attention_tally, value_size)
    stabs = jnp.moveaxis(stabs, 0, 1).reshape(attention_tally, rows)
    running = jnp.cumsum(forget_log, axis=1)
    return (raw, stabs, running, memory_end, level_end, running[:, -1])


def merge_states(earlier, later):
    merged = []
    for group in range(2):
        memory_e, level_e, total_e = earlier[3 * group : 3 * group + 3]
        memory_l, level_l, total_l = later[3 * group : 3 * group + 3]
        level = jnp.maximum(level_e + total_l, level_l)
        memory = (
            jnp.exp(level_e + total_l - level)[:, None, None] * memory_e
            + jnp.exp(level_l - level)[:, None, None] * memory_l
        )
        merged.extend([memory, level, total_e + total_l])
    return tuple(merged)


def finish_group(query, raw, stabs, running, memory_in, level_in, gain, outgate, key_size):
    rows, attention_tally, value_size = raw.shape
    shifted = running + level_in[:, None]
    stab = jnp.maximum(stabs, shifted)
    own = raw * jnp.exp(stabs - stab).T[:, :, None]
    queries = query.reshape(rows, attention_tally, key_size).astype(jnp.float32)
    incoming = jnp.einsum("thd,hdv->thv", queries, memory_in, precision=lax.Precision.HIGHEST)
    total = own + incoming * jnp.exp(shifted - stab).T[:, :, None]
    normal_raw = total * lax.rsqrt(jnp.mean(total * total, axis=-1, keepdims=True) + 1e-06)
    flat = normal_raw.reshape(rows, attention_tally * value_size)
    flat = flat * gain.astype(jnp.float32) * jax.nn.sigmoid(outgate.astype(jnp.float32))
    return flat.astype(jnp.bfloat16)


def norm_rows(middle_f, norm_gain):
    normed = middle_f * lax.rsqrt(jnp.mean(middle_f * middle_f, axis=-1, keepdims=True) + 1e-06)
    return (normed * norm_gain.astype(jnp.float32)).astype(jnp.bfloat16)


def body(
    residual,
    query_wide,
    key_wide,
    value_wide,
    outgate_wide,
    gating_wide,
    gain_wide,
    readout_wide,
    query_narrow,
    key_narrow,
    value_narrow,
    outgate_narrow,
    gating_narrow,
    gain_narrow,
    readout_narrow,
    norm_gain,
    gate_weight,
    up_weight,
    down_weight,
):
    raw_w, stabs_w, running_w, memory_w, level_w, total_w = local_pass(
        query_wide, key_wide, value_wide, gating_wide, DK_A
    )
    raw_n, stabs_n, running_n, memory_n, level_n, total_n = local_pass(
        query_narrow, key_narrow, value_narrow, gating_narrow, DK_B
    )
    carried = entering(
        (memory_w, level_w, total_w, memory_n, level_n, total_n),
        "sp",
        merge_states,
        (
            jnp.zeros_like(memory_w),
            jnp.full_like(level_w, -1e30),
            jnp.zeros_like(total_w),
            jnp.zeros_like(memory_n),
            jnp.full_like(level_n, -1e30),
            jnp.zeros_like(total_n),
        ),
    )
    gated_w = finish_group(
        query_wide, raw_w, stabs_w, running_w, carried[0], carried[1], gain_wide, outgate_wide, DK_A
    )
    gated_n = finish_group(
        query_narrow,
        raw_n,
        stabs_n,
        running_n,
        carried[3],
        carried[4],
        gain_narrow,
        outgate_narrow,
        DK_B,
    )
    mixed = lax.psum_scatter(
        (
            jnp.dot(gated_w, readout_wide, preferred_element_type=jnp.float32)
            + jnp.dot(gated_n, readout_narrow, preferred_element_type=jnp.float32)
        ).astype(jnp.bfloat16),
        "tp",
        scatter_dimension=0,
        tiled=True,
    ).astype(jnp.float32)
    middle_f = (residual.astype(jnp.float32) + mixed).astype(jnp.bfloat16).astype(jnp.float32)
    normed = norm_rows(middle_f, norm_gain)
    all_rows = lax.all_gather(normed, "tp", axis=0, tiled=True)
    gate = jnp.dot(
        all_rows,
        lax.all_gather(gate_weight, "sp", axis=0, tiled=True),
        preferred_element_type=jnp.float32,
    )
    upper = jnp.dot(
        all_rows,
        lax.all_gather(up_weight, "sp", axis=0, tiled=True),
        preferred_element_type=jnp.float32,
    )
    hidden = (jax.nn.silu(gate) * upper).astype(jnp.bfloat16)
    terms = jnp.dot(
        hidden,
        lax.all_gather(down_weight, "sp", axis=1, tiled=True),
        preferred_element_type=jnp.float32,
    )
    back = lax.psum_scatter(
        terms.astype(jnp.bfloat16), "tp", scatter_dimension=0, tiled=True
    ).astype(jnp.float32)
    return (middle_f + back).astype(jnp.bfloat16)


def solution(mesh):
    in_specs = (
        P(("sp", "tp"), None),
        P("sp", "tp"),
        P("sp", "tp"),
        P("sp", "tp"),
        P("sp", "tp"),
        P(None, "tp", "sp"),
        P("tp"),
        P("tp", None),
        P("sp", "tp"),
        P("sp", "tp"),
        P("sp", "tp"),
        P("sp", "tp"),
        P(None, "tp", "sp"),
        P("tp"),
        P("tp", None),
        P(),
        P("sp", "tp"),
        P("sp", "tp"),
        P("tp", "sp"),
    )
    out_specs = P(("sp", "tp"), None)
    return jax.shard_map(body, mesh=mesh, in_specs=in_specs, out_specs=out_specs, check_vma=False)
```

profile of v0, /device:TPU:0, one launch (start us, length us, event | category | flops | bytes accessed | tf_op | source)
XLA Modules:
  0.0 764.9 jit_solution(13011065428079746588)
XLA Ops:
  10.6 5.3 while.55
  19.7 19.3 %while.54 = (s32[]{:T(128)}, f32[4,128,256]{2,1,0:T(8,128)S(1)}, f32[4]{0:T(128)}, f32[2,64,4,256]{3,1,0,2:T(8,128)}, f32[2,4,64]{2,1,0:T(4,128)}, /*index=5*/f3...) while((s32[]{:T(128)}, f32[4,128,256]{2,1,0:T(8,128)S(1)}, ...), condition=%wide.region_4.5_spmd.clone, body=%wide.region_0.4_spmd.clone.sunk | while | flops 130980880 | bytes 3455009 | solution.py:75
  21.8 1.3 add_maximum_fusion.4
  27.8 1.3 fusion.153
  31.8 1.3 add_maximum_fusion.4
  37.8 1.2 fusion.153
  40.0 1.6 copy.70
  41.5 1.3 dynamic-slice
  48.0 44.1 %all-reduce.4 = (f32[64]{0:T(128)S(1)}, f32[64]{0:T(128)S(1)}, f32[64]{0:T(128)S(1)}, f32[64]{0:T(128)S(1)}) all-reduce(f32[64]{0:T(128)S(1)} %dynamic-update-slice, f32[64]{0:T(128)S(1)} %dynamic-update-slice.1, f32[64]{0:T(128)S(1)} %dynamic-update-slice.2, f32[64]{0:T(128)S(1)} %dynamic-update-slice.3), channel_id=2, replica_groups=mesh['sp'=16,'tp'=2] {'sp'}, use_global_device_ids=true, to_apply=%add | all-reduce | flops 256 | bytes 2048
  97.4 1.2 copy.63
  98.7 1.3 convert_element_type.74
  99.9 1.3 convert_element_type.77
  101.2 93.0 %all-gather.18.cloned.1.call-done = f32[64,128,256]{2,1,0:T(8,128)} async-done(((f32[4,128,256]{2,1,0:T(8,128)}), f32[64,128,256]{2,1,0:T(8,128)}) %all-gather.18.cloned.1.call-update) | async-done | bytes 8388624 | tf_op jit(solution)/shard_map/all_gather | solution.py:13
  194.2 56.7 %while.56 = (s32[]{:T(128)}, f32[4,128,256]{2,1,0:T(8,128)S(1)}, f32[4]{0:T(128)}, f32[4,64,128]{2,1,0:T(8,128)S(1)}, f32[4]{0:T(128)}, /*index=5*/s32[]{:T(128)...) while((s32[]{:T(128)}, f32[4,128,256]{2,1,0:T(8,128)S(1)}, ...), condition=%wide.region_13.14_spmd.clone, body=%wide.region_12.13_spmd.clone.sunk | while | flops 819260 | bytes 1966609 | solution.py:25
  194.2 1.3 broadcast_select_fusion.9
  195.5 1.2 fusion.162
  197.8 1.3 broadcast_select_fusion.9
  199.1 1.2 fusion.162
  201.3 1.3 broadcast_select_fusion.9
  202.6 1.2 fusion.162
  204.9 1.3 broadcast_select_fusion.9
  206.2 1.2 fusion.162
  208.4 1.3 broadcast_select_fusion.9
  209.7 1.2 fusion.162
  212.0 1.3 broadcast_select_fusion.9
  215.5 1.3 broadcast_select_fusion.9
  219.1 1.3 broadcast_select_fusion.9
  222.6 1.3 broadcast_select_fusion.9
  226.2 1.3 broadcast_select_fusion.9
  229.7 1.3 broadcast_select_fusion.9
  233.2 1.3 broadcast_select_fusion.9
  236.8 1.3 broadcast_select_fusion.9
  240.3 1.3 broadcast_select_fusion.9
  243.9 1.3 broadcast_select_fusion.9
  247.4 1.3 broadcast_select_fusion.9
  251.8 1.3 multiply_reduce_fusion.1
  254.8 1.5 multiply_reduce_fusion
  256.7 3.0 fusion.76
  259.8 1.3 fusion.67
  262.9 4.4 reduce-scatter.3.cloned.1.call-done
  269.6 2.4 all_gather.52
  272.0 140.6 %all-gather.12.cloned.1.call-done = bf16[2048,2816]{1,0:T(8,128)(2,1)} async-done(((bf16[128,2816]{1,0:T(8,128)(2,1)}), bf16[2048,2816]{1,0:T(8,128)(2,1)}) %all-gather.12.cloned.1.call-update) | async-done | bytes 11534352 | tf_op jit(solution)/shard_map/all_gather | solution.py:185
  412.5 7.1 fusion.118
  419.6 135.2 %all-gather.14.cloned.1.call-done = bf16[2048,2816]{1,0:T(8,128)(2,1)} async-done(((bf16[128,2816]{1,0:T(8,128)(2,1)}), bf16[2048,2816]{1,0:T(8,128)(2,1)}) %all-gather.14.cloned.1.call-update) | async-done | bytes 11534352 | tf_op jit(solution)/shard_map/all_gather | solution.py:190
  554.8 182.8 %all-gather.16.cloned.1.call-done = bf16[2816,2048]{1,0:T(8,128)(2,1)} async-done(((bf16[2816,128]{1,0:T(8,128)(2,1)}), bf16[2816,2048]{1,0:T(8,128)(2,1)}) %all-gather.16.cloned.1.call-update) | async-done | bytes 11534352 | tf_op jit(solution)/shard_map/all_gather | solution.py:196
  737.6 12.4 %convolution_convert_fusion = bf16[128,2048]{1,0:T(8,128)(2,1)} fusion(bf16[2816,2048]{1,0:T(8,128)(2,1)} %all-gather.16.cloned.1.call-done, bf16[128,2048]{1,0:T(8,128)(2,1)S(1)} %all_gather.52, bf16[2048,2816]{1,0:T(8,128)(2,1)} %all-gather.14.cloned.1.call-done, f32[128,2816]{1,0:T(8,128)} %fusion.118), kind=kOutput, calls=%fused_computation.130 | convolution fusion | flops 2955214848 | bytes 25559040 | tf_op jit(solution)/shard_map/dot_general | solution.py:194
  750.0 6.3 reduce-scatter.5.cloned.1.call-done
  756.3 1.7 fusion.75
  (240 shorter events, 74.2 us)
Async XLA Ops:
  6.5 253.2 %copy-start = (bf16[512,2048]{1,0:T(8,128)(2,1)S(1)}, bf16[512,2048]{1,0:T(8,128)(2,1)}, u32[]{:S(2)}) copy-start(bf16[512,2048]{1,0:T(8,128)(2,1)} %param.39) | copy-start | bytes 6291460
  6.5 94.7 %all-gather.20.cloned.1.call-start = ((), (), s32[]{:S(2)}) async-start(), calls=%async_computation.8 | async-start | bytes 2228224 | tf_op jit(solution)/shard_map/all_gather | solution.py:13
  10.6 6.1 copy-start.15
  10.6 7.0 copy-start.8
  10.6 7.1 copy-start.11
  10.6 7.2 copy-start.7
  15.9 0.6 copy-start.3
  15.9 1.6 copy-start.12
  15.9 1.6 copy-start.16
  16.6 177.6 %all-gather.18.cloned.1.call-start = ((), (), s32[]{:S(2)}) async-start(), calls=%async_computation.7 | async-start | bytes 8912896 | tf_op jit(solution)/shard_map/all_gather | solution.py:13
  20.4 2.7 copy-start.6
  21.0 2.1 copy-start.9
  29.8 3.3 copy-start.6
  31.0 2.1 copy-start.9
  39.0 0.8 copy-start.2
  39.9 227.5 %reduce-scatter.3.cloned.1.call-start = ((), (), s32[]{:S(2)}) async-start(), calls=%async_computation.2 | async-start | bytes 786432 | tf_op jit(solution)/shard_map/reduce_scatter | solution.py:171
  46.1 51.3 %copy-start.13 = (f32[4,128]{1,0:T(4,128)}, f32[4,128]{1,0:T(4,128)S(1)}, u32[]{:S(2)}) copy-start(f32[4,128]{1,0:T(4,128)S(1)} %reduce_window_sum.38) | copy-start | bytes 6148
  47.5 49.9 %copy-start.14 = (f32[4,128]{1,0:T(4,128)}, f32[4,128]{1,0:T(4,128)S(1)}, u32[]{:S(2)}) copy-start(f32[4,128]{1,0:T(4,128)S(1)} %reduce_window_sum.39) | copy-start | bytes 6148
  251.0 5.7 copy-start.19
  256.4 3.3 copy-start.10
  256.4 3.3 copy-start.17
  259.7 3.2 copy-start.18
  259.7 7.6 copy-start.4
  261.1 151.4 %all-gather.12.cloned.1.call-start = ((), (), s32[]{:S(2)}) async-start(), calls=%async_computation.3 | async-start | bytes 12255232 | tf_op jit(solution)/shard_map/all_gather | solution.py:185
  261.7 293.1 %all-gather.14.cloned.1.call-start = ((), (), s32[]{:S(2)}) async-start(), calls=%async_computation.4 | async-start | bytes 12255232 | tf_op jit(solution)/shard_map/all_gather | solution.py:190
  262.3 475.3 %all-gather.16.cloned.1.call-start = ((), (), s32[]{:S(2)}) async-start(), calls=%async_computation.5 | async-start | bytes 12255232 | tf_op jit(solution)/shard_map/all_gather | solution.py:196
  262.8 493.5 %reduce-scatter.5.cloned.1.call-start = ((), (), s32[]{:S(2)}) async-start(), calls=%async_computation.6 | async-start | bytes 786432 | tf_op jit(solution)/shard_map/reduce_scatter | solution.py:199
  419.6 336.7 %copy-start.5 = (bf16[64,2048]{1,0:T(8,128)(2,1)S(1)}, bf16[64,2048]{1,0:T(8,128)(2,1)}, u32[]{:S(2)}) copy-start(bf16[64,2048]{1,0:T(8,128)(2,1)} %reduce-scatter.3.cloned.1.call-done) | copy-start | bytes 786436
  737.6 20.5 %copy-start.1 = (bf16[512,2048]{1,0:T(8,128)(2,1)S(1)}, bf16[512,2048]{1,0:T(8,128)(2,1)}, u32[]{:S(2)}) copy-start(bf16[512,2048]{1,0:T(8,128)(2,1)} %param.39) | copy-start | bytes 6291460
Sparse Core Ops, SparseCore 0:
  16.7 63.6 all-gather.19
  83.2 111.0 all-gather.17
  261.2 6.0 reduce-scatter.2
  270.0 142.5 all-gather.11
  415.1 139.5 all-gather.13
  557.3 180.2 all-gather.15
  750.2 6.0 reduce-scatter.4
where the time goes:
time: 768 us; the launch traced here: 765 us
  waiting for transfers between devices  564 us (73%)
  other arithmetic  79.1 us (10%)
  blocking collectives  46.5 us (6%)
  matrix products  35.6 us (5%)
  local copies, waits for them, and re-layouts  24.3 us (3%)
  between operations  14.5 us (2%)
    all_gather x1, waiting for transfers between devices, body(): lax.all_gather(down_weight, 'sp', axis=1, tiled=True)  183 us
    all_gather x1, waiting for transfers between devices, body(): lax.all_gather(gate_weight, 'sp', axis=0, tiled=True)  141 us
    all_gather x1, waiting for transfers between devices, body(): lax.all_gather(up_weight, 'sp', axis=0, tiled=True)  135 us
    all_gather x2, waiting for transfers between devices, entering(): everything = jax.tree.map(lambda part: lax.all_gather(part, axis), value)  93 us
    select_n x48, other arithmetic, step(): return jax.tree.map(lambda a, b: jnp.where(reached, a, b), new, before)  55.7 us
    unnamed x1, blocking collectives  44.1 us
  transfers between devices with their start and end apart: 7, of which 6 were waited for; matrix products, arithmetic and copies ran while one was open for 6% of the time, Pallas kernels for 0%

commit v1 on v0

--- a/solution.py
+++ b/solution.py
@@ -182,7 +182,9 @@
     all_rows = lax.all_gather(normed, "tp", axis=0, tiled=True)
     gate = jnp.dot(
         all_rows,
-        lax.all_gather(gate_weight, "sp", axis=0, tiled=True),
+        jnp.concatenate(
+            lax.all_to_all(jnp.stack([gate_weight] * lax.axis_size("sp")), "sp", 0, 0), axis=0
+        ),
         preferred_element_type=jnp.float32,
     )
     upper = jnp.dot(

time: 768 us -> 836 us (1.089)
  waiting for transfers between devices: 564 us -> 622 us
    all_to_all x0 -> x1, waiting for transfers between devices: none -> 260 us  [body(): lax.all_to_all(jnp.stack([gate_weight] * lax.axis_size('sp')), 'sp', 0, 0)]
    all_gather x1 -> x0, waiting for transfers between devices: 141 us -> none  [body(): lax.all_gather(gate_weight, 'sp', axis=0, tiled=True)]
    all_gather x1, waiting for transfers between devices: 135 us -> 71.1 us  [body(): lax.all_gather(up_weight, 'sp', axis=0, tiled=True)]
  transfers between devices with their start and end apart: 7 -> 7, of which waited for: 6 -> 5; matrix products, arithmetic and copies ran while one was open for 6% -> 6% of each run, Pallas kernels for 0% -> 0%
where the time goes in v1:
time: 836 us; the launch traced here: 833 us
  waiting for transfers between devices  622 us (74%)
  other arithmetic  79.1 us (9%)
  blocking collectives  46.5 us (6%)
  matrix products  35.6 us (4%)
  local copies, waits for them, and re-layouts  29.6 us (4%)
  between operations  14.6 us (2%)
    all_to_all x1, waiting for transfers between devices, body(): lax.all_to_all(jnp.stack([gate_weight] * lax.axis_size('sp')), 'sp', 0, 0)  260 us
    all_gather x1, waiting for transfers between devices, body(): lax.all_gather(down_weight, 'sp', axis=1, tiled=True)  191 us
    all_gather x2, waiting for transfers between devices, entering(): everything = jax.tree.map(lambda part: lax.all_gather(part, axis), value)  93 us
    all_gather x1, waiting for transfers between devices, body(): lax.all_gather(up_weight, 'sp', axis=0, tiled=True)  71.1 us
    select_n x48, other arithmetic, step(): return jax.tree.map(lambda a, b: jnp.where(reached, a, b), new, before)  55.7 us
    unnamed x1, blocking collectives  44.1 us
  transfers between devices with their start and end apart: 7, of which 5 were waited for; matrix products, arithmetic and copies ran while one was open for 6% of the time, Pallas kernels for 0%

profile of v1, /device:TPU:0, one launch (start us, length us, event | category | flops | bytes accessed | tf_op | source)
XLA Modules:
  0.0 833.5 jit_solution(12622609114890847662)
XLA Ops:
  10.6 5.3 while.55
  19.7 19.3 %while.54 = (s32[]{:T(128)}, f32[4,128,256]{2,1,0:T(8,128)S(1)}, f32[4]{0:T(128)}, f32[2,64,4,256]{3,1,0,2:T(8,128)}, f32[2,4,64]{2,1,0:T(4,128)}, /*index=5*/f3...) while((s32[]{:T(128)}, f32[4,128,256]{2,1,0:T(8,128)S(1)}, ...), condition=%wide.region_4.5_spmd.clone, body=%wide.region_0.4_spmd.clone.sunk | while | flops 130980880 | bytes 3455009 | solution.py:75
  21.8 1.3 add_maximum_fusion.4
  27.8 1.3 fusion.153
  31.8 1.3 add_maximum_fusion.4
  37.8 1.2 fusion.153
  40.0 1.6 copy.70
  41.5 1.3 dynamic-slice
  48.0 44.1 %all-reduce.4 = (f32[64]{0:T(128)S(1)}, f32[64]{0:T(128)S(1)}, f32[64]{0:T(128)S(1)}, f32[64]{0:T(128)S(1)}) all-reduce(f32[64]{0:T(128)S(1)} %dynamic-update-slice, f32[64]{0:T(128)S(1)} %dynamic-update-slice.1, f32[64]{0:T(128)S(1)} %dynamic-update-slice.2, f32[64]{0:T(128)S(1)} %dynamic-update-slice.3), channel_id=2, replica_groups=mesh['sp'=16,'tp'=2] {'sp'}, use_global_device_ids=true, to_apply=%add | all-reduce | flops 256 | bytes 2048
  97.4 1.2 copy.63
  98.7 1.3 convert_element_type.74
  99.9 1.3 convert_element_type.77
  101.2 93.0 %all-gather.15.cloned.1.call-done = f32[64,128,256]{2,1,0:T(8,128)} async-done(((f32[4,128,256]{2,1,0:T(8,128)}), f32[64,128,256]{2,1,0:T(8,128)}) %all-gather.15.cloned.1.call-update) | async-done | bytes 8388624 | tf_op jit(solution)/shard_map/all_gather | solution.py:13
  194.2 56.7 %while.56 = (s32[]{:T(128)}, f32[4,128,256]{2,1,0:T(8,128)S(1)}, f32[4]{0:T(128)}, f32[4,64,128]{2,1,0:T(8,128)S(1)}, f32[4]{0:T(128)}, /*index=5*/s32[]{:T(128)...) while((s32[]{:T(128)}, f32[4,128,256]{2,1,0:T(8,128)S(1)}, ...), condition=%wide.region_13.14_spmd.clone, body=%wide.region_12.13_spmd.clone.sunk | while | flops 819260 | bytes 1966609 | solution.py:25
  194.2 1.3 broadcast_select_fusion.9
  195.5 1.2 fusion.162
  197.8 1.3 broadcast_select_fusion.9
  199.1 1.2 fusion.162
  201.3 1.3 broadcast_select_fusion.9
  202.6 1.2 fusion.162
  204.9 1.3 broadcast_select_fusion.9
  206.2 1.2 fusion.162
  208.4 1.3 broadcast_select_fusion.9
  212.0 1.3 broadcast_select_fusion.9
  215.5 1.3 broadcast_select_fusion.9
  219.1 1.3 broadcast_select_fusion.9
  222.6 1.3 broadcast_select_fusion.9
  226.2 1.3 broadcast_select_fusion.9
  229.7 1.3 broadcast_select_fusion.9
  233.2 1.3 broadcast_select_fusion.9
  236.8 1.3 broadcast_select_fusion.9
  240.3 1.3 broadcast_select_fusion.9
  243.9 1.3 broadcast_select_fusion.9
  247.4 1.3 broadcast_select_fusion.9
  251.8 1.3 multiply_reduce_fusion.1
  254.8 1.5 multiply_reduce_fusion
  256.7 3.0 fusion.76
  259.7 1.3 fusion.67
  261.7 5.3 stack.2
  266.9 5.0 all-to-all-start
  274.9 2.4 all_gather.49
  277.2 259.9 %all-to-all-done = bf16[16,128,2816]{2,1,0:T(8,128)(2,1)} async-done(((bf16[16,128,2816]{2,1,0:T(8,128)(2,1)}), bf16[16,128,2816]{2,1,0:T(8,128)(2,1)}, u32[]{:S(2)}, u32[]{:S(2)}) %all-to-all-start) | async-done | bytes 11534368 | tf_op jit(solution)/shard_map/all_to_all | solution.py:186
  537.2 7.1 fusion.118
  544.2 71.1 %all-gather.11.cloned.1.call-done = bf16[2048,2816]{1,0:T(8,128)(2,1)} async-done(((bf16[128,2816]{1,0:T(8,128)(2,1)}), bf16[2048,2816]{1,0:T(8,128)(2,1)}) %all-gather.11.cloned.1.call-update) | async-done | bytes 11534352 | tf_op jit(solution)/shard_map/all_gather | solution.py:192
  615.4 190.7 %all-gather.13.cloned.1.call-done = bf16[2816,2048]{1,0:T(8,128)(2,1)} async-done(((bf16[2816,128]{1,0:T(8,128)(2,1)}), bf16[2816,2048]{1,0:T(8,128)(2,1)}) %all-gather.13.cloned.1.call-update) | async-done | bytes 11534352 | tf_op jit(solution)/shard_map/all_gather | solution.py:198
  806.1 12.4 %convolution_convert_fusion = bf16[128,2048]{1,0:T(8,128)(2,1)} fusion(bf16[2816,2048]{1,0:T(8,128)(2,1)} %all-gather.13.cloned.1.call-done, bf16[128,2048]{1,0:T(8,128)(2,1)S(1)} %all_gather.49, bf16[2048,2816]{1,0:T(8,128)(2,1)} %all-gather.11.cloned.1.call-done, f32[128,2816]{1,0:T(8,128)} %fusion.118), kind=kOutput, calls=%fused_computation.130 | convolution fusion | flops 2955214848 | bytes 25559040 | tf_op jit(solution)/shard_map/dot_general | solution.py:196
  818.6 6.3 reduce-scatter.5.cloned.1.call-done
  824.9 1.7 fusion.75
  (242 shorter events, 74.8 us)
Async XLA Ops:
  6.5 253.2 %copy-start = (bf16[512,2048]{1,0:T(8,128)(2,1)S(1)}, bf16[512,2048]{1,0:T(8,128)(2,1)}, u32[]{:S(2)}) copy-start(bf16[512,2048]{1,0:T(8,128)(2,1)} %param.39) | copy-start | bytes 6291460
  6.5 94.7 %all-gather.17.cloned.1.call-start = ((), (), s32[]{:S(2)}) async-start(), calls=%async_computation.8 | async-start | bytes 2228224 | tf_op jit(solution)/shard_map/all_gather | solution.py:13
  10.6 6.1 copy-start.16
  10.6 7.0 copy-start.9
  10.6 7.1 copy-start.12
  10.6 7.2 copy-start.8
  15.9 0.6 copy-start.3
  15.9 1.6 copy-start.13
  15.9 1.6 copy-start.17
  16.6 177.6 %all-gather.15.cloned.1.call-start = ((), (), s32[]{:S(2)}) async-start(), calls=%async_computation.7 | async-start | bytes 8912896 | tf_op jit(solution)/shard_map/all_gather | solution.py:13
  20.4 2.7 copy-start.6
  21.0 2.1 copy-start.10
  29.8 3.3 copy-start.6
  31.0 2.1 copy-start.10
  39.0 0.8 copy-start.2
  39.9 232.8 %reduce-scatter.3.cloned.1.call-start = ((), (), s32[]{:S(2)}) async-start(), calls=%async_computation.3 | async-start | bytes 786432 | tf_op jit(solution)/shard_map/reduce_scatter | solution.py:171
  46.1 51.3 %copy-start.14 = (f32[4,128]{1,0:T(4,128)}, f32[4,128]{1,0:T(4,128)S(1)}, u32[]{:S(2)}) copy-start(f32[4,128]{1,0:T(4,128)S(1)} %reduce_window_sum.38) | copy-start | bytes 6148
  47.5 49.9 %copy-start.15 = (f32[4,128]{1,0:T(4,128)}, f32[4,128]{1,0:T(4,128)S(1)}, u32[]{:S(2)}) copy-start(f32[4,128]{1,0:T(4,128)S(1)} %reduce_window_sum.39) | copy-start | bytes 6148
  251.0 5.7 copy-start.20
  256.4 3.3 copy-start.11
  256.4 3.3 copy-start.18
  259.7 1.9 copy-start.7
  261.1 354.3 %all-gather.11.cloned.1.call-start = ((), (), s32[]{:S(2)}) async-start(), calls=%async_computation.4 | async-start | bytes 12255232 | tf_op jit(solution)/shard_map/all_gather | solution.py:192
  266.9 5.7 copy-start.19
  266.9 5.7 copy-start.4
  266.9 270.2 %all-to-all-start = ((bf16[16,128,2816]{2,1,0:T(8,128)(2,1)}), bf16[16,128,2816]{2,1,0:T(8,128)(2,1)}, u32[]{:S(2)}, u32[]{:S(2)}) async-start(bf16[16,128,2816]{2,1,0:T(8,128)(2,1)} %stack.2), calls=%async_computation.1 | async-start | bytes 23068672 | tf_op jit(solution)/shard_map/all_to_all | solution.py:186
  272.0 534.2 %all-gather.13.cloned.1.call-start = ((), (), s32[]{:S(2)}) async-start(), calls=%async_computation.5 | async-start | bytes 12255232 | tf_op jit(solution)/shard_map/all_gather | solution.py:198
  272.5 552.3 %reduce-scatter.5.cloned.1.call-start = ((), (), s32[]{:S(2)}) async-start(), calls=%async_computation.6 | async-start | bytes 786432 | tf_op jit(solution)/shard_map/reduce_scatter | solution.py:201
  544.2 280.6 %copy-start.5 = (bf16[64,2048]{1,0:T(8,128)(2,1)S(1)}, bf16[64,2048]{1,0:T(8,128)(2,1)}, u32[]{:S(2)}) copy-start(bf16[64,2048]{1,0:T(8,128)(2,1)} %reduce-scatter.3.cloned.1.call-done) | copy-start | bytes 786436
  806.1 20.5 %copy-start.1 = (bf16[512,2048]{1,0:T(8,128)(2,1)S(1)}, bf16[512,2048]{1,0:T(8,128)(2,1)}, u32[]{:S(2)}) copy-start(bf16[512,2048]{1,0:T(8,128)(2,1)} %param.39) | copy-start | bytes 6291460
Sparse Core Ops, SparseCore 0:
  16.7 63.6 all-gather.16
  83.2 111.0 all-gather.14
  261.2 6.0 reduce-scatter.2
  269.9 345.3 all-gather.10
  617.9 188.1 all-gather.12
  818.7 6.0 reduce-scatter.4
